TPU v7x, 512 devices: a 4x2x32 block of a 4x8x32 slice. The times are simulated.
512 devices in a mesh: grp: 2 (over y), fs: 32 (over z), tp: 8 (over x, core).
Axes of the slice: x: 4, y: 2, z: 32, core: 2. Of those that a mesh axis runs over, the one named last changes fastest.
The devices are a block of a 4x8x32 slice.
Arguments:
- prompt: bfloat16 [4096, 2048], P(('grp', 'tp')), parts along dimension 0, may hold values from -6 to 6
- gain_first: float32 [2048], P('fs'), may hold values from 0.1 to 1.9
- gate_first: float32 [2048, 4096], P('fs', 'tp'), may hold values from -0.125 to 0.125
- up_first: float32 [2048, 4096], P('fs', 'tp'), may hold values from -0.125 to 0.125
- down_first: float32 [4096, 2048], P('fs', 'tp'), may hold values from -0.09375 to 0.09375
- gain_second: float32 [2048], P('fs'), may hold values from 0.1 to 1.9
- gate_second: float32 [2048, 4096], P('fs', 'tp'), may hold values from -0.125 to 0.125
- up_second: float32 [2048, 4096], P('fs', 'tp'), may hold values from -0.125 to 0.125
- down_second: float32 [4096, 2048], P('fs', 'tp'), may hold values from -0.09375 to 0.09375
Outputs:
- result: bfloat16 [4096, 2048], P(('grp', 'tp')), parts along dimension 0
- served_gate_first: bfloat16 [4096, 4096], P('grp', 'fs'), parts along dimension 0
- served_up_first: bfloat16 [4096, 4096], P('grp', 'fs'), parts along dimension 0
- served_down_first: bfloat16 [4096, 4096], P('fs', 'grp'), parts along dimension 1
- served_gate_second: bfloat16 [4096, 4096], P('grp', 'fs'), parts along dimension 0
- served_up_second: bfloat16 [4096, 4096], P('grp', 'fs'), parts along dimension 0
- served_down_second: bfloat16 [4096, 4096], P('fs', 'grp'), parts along dimension 1
There are 2 independent parts, one for each index of `grp`. A program takes and returns all parts, laid end to end along the dimension named above; an argument that names none is the same for every part. Nothing has to cross between parts.
All inputs are finite; a program needn't handle non-finite values.
Results may differ from a plain program's by a relative error of at most 0.0053.
Values may be sent and summed in bfloat16 or wider, within the bound.
A program may use at most 64 MiB of HBM per device.

v0:
```python
import jax
import jax.numpy as jnp
from jax import lax
from jax.sharding import PartitionSpec as P

EPS = 1e-06


def as_sent(array):
    return jax.tree.map(lambda a: a.astype(jnp.bfloat16) if a.dtype == jnp.float32 else a, array)


def in_order(blocks, dim):
    blocks = jnp.moveaxis(blocks, 0, dim)
    lengths = blocks.shape
    return blocks.reshape(*lengths[:dim], lengths[dim] * lengths[dim + 1], *lengths[dim + 2 :])


def copy_for_each(array, axis):
    copies = jnp.broadcast_to(array, (lax.axis_size(axis), *array.shape))
    return lax.all_to_all(copies, axis, split_axis=0, concat_axis=0, tiled=True)


def gather_directly(array, axis, dim):
    return in_order(copy_for_each(array, axis), dim)


def in_one_piece(arrays, axis, dim, along):
    widths = [a.shape[along] for a in arrays]
    both = jnp.concatenate(arrays, axis=along)
    out = lax.all_gather(both, axis, axis=dim, tiled=True)
    return tuple(jnp.split(out, [sum(widths[:k]) for k in range(1, len(widths))], axis=along))


def fold(gain, weight):
    return (gain[:, None] * weight).astype(jnp.bfloat16)


def normed_of(stream):
    return (stream * lax.rsqrt(jnp.mean(stream * stream, axis=-1, keepdims=True) + EPS)).astype(
        jnp.bfloat16
    )


def hidden_of(normed, w_gate, w_up):
    gate = jnp.dot(normed, w_gate, preferred_element_type=jnp.float32)
    up_val = jnp.dot(normed, w_up, preferred_element_type=jnp.float32)
    return (jax.nn.silu(gate) * up_val).astype(jnp.bfloat16)


def on_device(
    prompt,
    gain_first,
    gate_first,
    up_first,
    down_first,
    gain_second,
    gate_second,
    up_second,
    down_second,
):
    folded = (
        fold(gain_first, gate_first),
        fold(gain_first, up_first),
        fold(gain_second, gate_second),
        fold(gain_second, up_second),
    )
    downs = (down_first.astype(jnp.bfloat16), down_second.astype(jnp.bfloat16))
    spread = (
        lax.all_to_all(folded[0], "tp", split_axis=0, concat_axis=1, tiled=True),
        lax.all_to_all(folded[1], "tp", split_axis=0, concat_axis=1, tiled=True),
        lax.all_to_all(folded[2], "tp", split_axis=0, concat_axis=1, tiled=True),
        lax.all_to_all(folded[3], "tp", split_axis=0, concat_axis=1, tiled=True),
    )
    moved = (
        lax.all_to_all(spread[0], "fs", split_axis=1, concat_axis=0, tiled=True),
        lax.all_to_all(spread[1], "fs", split_axis=1, concat_axis=0, tiled=True),
        lax.all_to_all(spread[2], "fs", split_axis=1, concat_axis=0, tiled=True),
        lax.all_to_all(spread[3], "fs", split_axis=1, concat_axis=0, tiled=True),
    )
    n_fs = lax.axis_size("fs")
    width = moved[0].shape[1]
    piece = moved[0].shape[0] // n_fs
    shaped = tuple((m.reshape(n_fs, piece, width) for m in moved))
    joined = jax.tree.map(
        lambda part, own: part.astype(own.dtype),
        jax.tree.map(lambda part: gather_directly(part, "tp", 1), as_sent(shaped)),
        shaped,
    )
    served = tuple((m.reshape(-1, width) for m in joined))
    served_downs = in_one_piece((downs[0], downs[1]), "tp", 1, 0)
    gates = (served[0], served[2])
    ups = (served[1], served[3])
    stream = prompt.astype(jnp.float32)
    for layer in range(2):
        hidden = hidden_of(normed_of(stream), gates[layer], ups[layer])
        partial_out = jnp.dot(hidden, served_downs[layer], preferred_element_type=jnp.float32)
        stream = stream + 0.5 * lax.psum(partial_out, "fs")
    result = stream.astype(jnp.bfloat16)
    return (result, served[0], served[1], served_downs[0], served[2], served[3], served_downs[1])


def solution(mesh):
    return jax.shard_map(
        on_device,
        mesh=mesh,
        in_specs=(
            P(("grp", "tp"), None),
            P("fs"),
            P("fs", "tp"),
            P("fs", "tp"),
            P("fs", "tp"),
            P("fs"),
            P("fs", "tp"),
            P("fs", "tp"),
            P("fs", "tp"),
        ),
        out_specs=(
            P(("grp", "tp"), None),
            P("grp", "fs"),
            P("grp", "fs"),
            P("fs", "grp"),
            P("grp", "fs"),
            P("grp", "fs"),
            P("fs", "grp"),
        ),
        check_vma=False,
    )
```

profile of v0, /device:TPU:40, one launch (start us, length us, event | category | flops | bytes accessed | tf_op | source)
XLA Modules:
  0.0 689.4 jit_solution(1443292288282662853)
XLA Ops:
  7.2 1.1 fusion.20
  8.3 10.1 %all_to_all.148 = bf16[8,8,512]{2,1,0:T(8,128)(2,1)} all-to-all(bf16[8,8,512]{2,1,0:T(8,128)(2,1)S(1)} %get-tuple-element.11), channel_id=1, replica_groups=mesh['grp'=2,'fs'=32,'tp'=8] {'tp'}, dimensions={0} | all-to-all | bytes 131072 | tf_op jit(solution)/shard_map/all_to_all | solution.py:70
  18.4 8.0 %all_to_all.149 = bf16[8,8,512]{2,1,0:T(8,128)(2,1)S(1)} all-to-all(bf16[8,8,512]{2,1,0:T(8,128)(2,1)S(1)} %get-tuple-element.12), channel_id=1, replica_groups=mesh['grp'=2,'fs'=32,'tp'=8] {'tp'}, dimensions={0} | all-to-all | bytes 131072 | tf_op jit(solution)/shard_map/all_to_all | solution.py:71
  26.4 45.8 %all-to-all-start.1 = ((bf16[8,32,128]{2,0,1:T(8,128)(2,1)}), bf16[8,32,128]{2,0,1:T(8,128)(2,1)S(1)}, u32[]{:S(2)}, u32[]{:S(2)}) async-start(bf16[8,32,128]{2,0,1:T(8,128)(2,1)} %bitcast.2), calls=%async_computation.1 | async-start | bytes 131072 | tf_op jit(solution)/shard_map/all_to_all | solution.py:76
  72.2 0.1 all-gather.2.cloned.1.call-start
  72.3 1.0 convert_element_type.41
  73.3 0.9 convert_element_type.42
  74.2 0.7 pad_maximum_fusion
  74.8 0.1 all-gather.2.cloned.1.call-update
  74.9 22.3 %all-to-all-done.1 = bf16[8,32,128]{2,0,1:T(8,128)(2,1)S(1)} async-done(((bf16[8,32,128]{2,0,1:T(8,128)(2,1)}), bf16[8,32,128]{2,0,1:T(8,128)(2,1)S(1)}, u32[]{:S(2)}, u32[]{:S(2)}) %all-to-all-start.1) | async-done | bytes 65568 | tf_op jit(solution)/shard_map/all_to_all | solution.py:76
  97.2 27.9 %all_to_all.150 = bf16[8,32,128]{2,0,1:T(8,128)(2,1)S(1)} all-to-all(bf16[8,32,128]{2,0,1:T(8,128)(2,1)S(1)} %bitcast.56), channel_id=1, replica_groups=mesh['grp'=2,'fs'=32,'tp'=8] {'fs'}, dimensions={1} | all-to-all | bytes 131072 | tf_op jit(solution)/shard_map/all_to_all | solution.py:77
  125.1 0.1 broadcast_in_dim.9
  125.2 12.8 %all_to_all.151 = bf16[8,32,8,128]{3,2,1,0:T(8,128)(2,1)S(1)} all-to-all(bf16[8,32,8,128]{3,2,1,0:T(8,128)(2,1)S(1)} %broadcast_in_dim.9), channel_id=1, replica_groups=mesh['grp'=2,'fs'=32,'tp'=8] {'tp'}, dimensions={0} | all-to-all | bytes 1048576 | tf_op jit(solution)/shard_map/all_to_all | solution.py:21
  138.0 0.9 broadcast_in_dim.8
  138.9 3.7 all-to-all-start.2
  142.6 0.1 all-reduce.3.cloned.1.call-start
  142.7 0.3 fusion
  143.0 0.1 copy.17
  143.1 9.6 %all-to-all-done.2 = bf16[8,32,8,128]{3,2,1,0:T(8,128)(2,1)S(1)} async-done(((bf16[8,32,8,128]{3,2,1,0:T(8,128)(2,1)}), bf16[8,32,8,128]{3,2,1,0:T(8,128)(2,1)S(1)}, u32[]{:S(2)}, u32[]{:S(2)}) %all-to-all-start.2) | async-done | bytes 524320 | tf_op jit(solution)/shard_map/all_to_all | solution.py:21
  152.7 0.1 copy.16
  152.8 0.8 copy-done.6
  153.6 0.5 fusion.8
  154.1 2.1 fusion.28
  156.2 2.2 fusion.5
  158.4 0.1 all-reduce.3.cloned.1.call-update
  158.5 0.8 copy-done.7
  159.3 0.1 copy-done.8
  159.4 0.1 fusion.22
  159.5 8.1 %all_to_all.152 = bf16[8,8,512]{2,1,0:T(8,128)(2,1)S(1)} all-to-all(bf16[8,8,512]{2,1,0:T(8,128)(2,1)S(1)} %get-tuple-element.9), channel_id=1, replica_groups=mesh['grp'=2,'fs'=32,'tp'=8] {'tp'}, dimensions={0} | all-to-all | bytes 131072 | tf_op jit(solution)/shard_map/all_to_all | solution.py:72
  167.5 8.0 %all_to_all.153 = bf16[8,8,512]{2,1,0:T(8,128)(2,1)S(1)} all-to-all(bf16[8,8,512]{2,1,0:T(8,128)(2,1)S(1)} %get-tuple-element.10), channel_id=1, replica_groups=mesh['grp'=2,'fs'=32,'tp'=8] {'tp'}, dimensions={0} | all-to-all | bytes 131072 | tf_op jit(solution)/shard_map/all_to_all | solution.py:73
  175.6 29.9 %all_to_all.154 = bf16[8,32,128]{2,0,1:T(8,128)(2,1)S(1)} all-to-all(bf16[8,32,128]{2,0,1:T(8,128)(2,1)S(1)} %bitcast.57), channel_id=1, replica_groups=mesh['grp'=2,'fs'=32,'tp'=8] {'fs'}, dimensions={1} | all-to-all | bytes 131072 | tf_op jit(solution)/shard_map/all_to_all | solution.py:78
  205.5 29.2 %all_to_all.155 = bf16[8,32,128]{2,0,1:T(8,128)(2,1)S(1)} all-to-all(bf16[8,32,128]{2,0,1:T(8,128)(2,1)S(1)} %bitcast.58), channel_id=1, replica_groups=mesh['grp'=2,'fs'=32,'tp'=8] {'fs'}, dimensions={1} | all-to-all | bytes 131072 | tf_op jit(solution)/shard_map/all_to_all | solution.py:79
  234.7 0.1 broadcast_in_dim.21
  234.8 12.8 %all_to_all.156 = bf16[8,32,8,128]{3,2,1,0:T(8,128)(2,1)S(1)} all-to-all(bf16[8,32,8,128]{3,2,1,0:T(8,128)(2,1)S(1)} %broadcast_in_dim.21), channel_id=1, replica_groups=mesh['grp'=2,'fs'=32,'tp'=8] {'tp'}, dimensions={0} | all-to-all | bytes 1048576 | tf_op jit(solution)/shard_map/all_to_all | solution.py:21
  247.6 0.9 broadcast_in_dim.20
  248.5 3.7 all-to-all-start.8
  252.2 0.1 all-reduce.5.cloned.1.call-start
  252.3 0.9 copy.19
  253.2 9.1 %all-to-all-done.8 = bf16[8,32,8,128]{3,2,1,0:T(8,128)(2,1)S(1)} async-done(((bf16[8,32,8,128]{3,2,1,0:T(8,128)(2,1)}), bf16[8,32,8,128]{3,2,1,0:T(8,128)(2,1)S(1)}, u32[]{:S(2)}, u32[]{:S(2)}) %all-to-all-start.8) | async-done | bytes 524320 | tf_op jit(solution)/shard_map/all_to_all | solution.py:21
  262.3 0.9 copy.18
  263.2 149.4 %all-reduce.3.cloned.1.call-done = f32[256,2048]{1,0:T(8,128)} async-done(((f32[256,2048]{1,0:T(8,128)}), f32[256,2048]{1,0:T(8,128)}) %all-reduce.3.cloned.1.call-update) | async-done | bytes 2097168 | tf_op jit(solution)/shard_map/psum | solution.py:98
  412.7 2.2 multiply_reduce_fusion
  414.9 0.3 multiply_convert_fusion
  415.2 1.0 copy-done.2
  416.2 0.4 fusion.29
  416.6 3.6 fusion.4
  420.3 259.4 %all-reduce.5.cloned.1.call-done = f32[256,2048]{1,0:T(8,128)} async-done(((f32[256,2048]{1,0:T(8,128)}), f32[256,2048]{1,0:T(8,128)}) %all-reduce.5.cloned.1.call-update) | async-done | bytes 2097168 | tf_op jit(solution)/shard_map/psum | solution.py:98
  679.7 3.1 add_convert_fusion
  (20 shorter events, 0.2 us)
Async XLA Ops:
  26.4 70.8 %all-to-all-start.1 = ((bf16[8,32,128]{2,0,1:T(8,128)(2,1)}), bf16[8,32,128]{2,0,1:T(8,128)(2,1)S(1)}, u32[]{:S(2)}, u32[]{:S(2)}) async-start(bf16[8,32,128]{2,0,1:T(8,128)(2,1)} %bitcast.2), calls=%async_computation.1 | async-start | bytes 131072 | tf_op jit(solution)/shard_map/all_to_all | solution.py:76
  72.2 70.5 %copy-start = (bf16[256,2048]{1,0:T(8,128)(2,1)S(1)}, bf16[256,2048]{1,0:T(8,128)(2,1)}, u32[]{:S(2)}) copy-start(bf16[256,2048]{1,0:T(8,128)(2,1)} %param.9) | copy-start | bytes 3145732
  72.2 81.9 %all-gather.2.cloned.1.call-start = ((), (), s32[]{:S(2)}) async-start(), calls=%async_computation.12 | async-start | bytes 1179648 | tf_op jit(solution)/shard_map/all_gather | solution.py:31
  138.9 13.8 %all-to-all-start.2 = ((bf16[8,32,8,128]{3,2,1,0:T(8,128)(2,1)}), bf16[8,32,8,128]{3,2,1,0:T(8,128)(2,1)S(1)}, u32[]{:S(2)}, u32[]{:S(2)}) async-start(bf16[8,32,8,128]{3,2,1,0:T(8,128)(2,1)} %broadcast_in_dim.8), calls=%async_computation.2 | async-start | bytes 1048576 | tf_op jit(solution)/shard_map/all_to_all | solution.py:21
  142.6 270.1 %all-reduce.3.cloned.1.call-start = ((), (), s32[]{:S(2)}) async-start(), calls=%async_computation.13 | async-start | bytes 4194304 | tf_op jit(solution)/shard_map/psum | solution.py:98
  143.1 13.1 %copy-start.3 = (bf16[8,32,8,128]{3,2,0,1:T(8,128)(2,1)}, bf16[8,32,8,128]{3,2,0,1:T(8,128)(2,1)S(1)}, u32[]{:S(2)}) copy-start(bf16[8,32,8,128]{3,2,0,1:T(8,128)(2,1)S(1)} %copy.17) | copy-start | bytes 1572868
  152.8 0.8 copy-start.6
  156.2 2.2 copy-start.4
  158.4 0.9 copy-start.7
  158.4 1.0 copy-start.8
  158.4 1.0 copy-start.9
  248.5 13.8 %all-to-all-start.8 = ((bf16[8,32,8,128]{3,2,1,0:T(8,128)(2,1)}), bf16[8,32,8,128]{3,2,1,0:T(8,128)(2,1)S(1)}, u32[]{:S(2)}, u32[]{:S(2)}) async-start(bf16[8,32,8,128]{3,2,1,0:T(8,128)(2,1)} %broadcast_in_dim.20), calls=%async_computation.8 | async-start | bytes 1048576 | tf_op jit(solution)/shard_map/all_to_all | solution.py:21
  252.2 427.5 %all-reduce.5.cloned.1.call-start = ((), (), s32[]{:S(2)}) async-start(), calls=%async_computation.14 | async-start | bytes 4194304 | tf_op jit(solution)/shard_map/psum | solution.py:98
  412.7 2.2 copy-start.1
  414.9 1.3 copy-start.5
  415.2 1.0 copy-start.2
Sparse Core Ops, SparseCore 0:
  75.7 37.6 all-gather.1
  158.6 254.0 all-reduce.2
  420.4 259.2 all-reduce.4
where the time goes:
time: 691 us; the launch traced here: 689 us
  waiting for transfers between devices  450 us (65%)
  blocking collectives  147 us (21%)
  starting transfers between devices  53.4 us (8%)
  between operations  13.9 us (2%)
  other arithmetic  9.56 us (1%)
  local copies, waits for them, and re-layouts  8.82 us (1%)
    psum x2, waiting for transfers between devices, on_device(): stream = stream + 0.5 * lax.psum(partial_out, 'fs')  409 us
    all_to_all x1, starting transfers between devices, on_device(): lax.all_to_all(spread[0], 'fs', split_axis=1, concat_axis=0, tiled=True)  45.8 us
    all_to_all x1, blocking collectives, on_device(): lax.all_to_all(spread[2], 'fs', split_axis=1, concat_axis=0, tiled=True)  29.9 us
    all_to_all x1, blocking collectives, on_device(): lax.all_to_all(spread[3], 'fs', split_axis=1, concat_axis=0, tiled=True)  29.2 us
    all_to_all x1, blocking collectives, on_device(): lax.all_to_all(spread[1], 'fs', split_axis=1, concat_axis=0, tiled=True)  27.9 us
    all_to_all x2, blocking collectives, copy_for_each(): return lax.all_to_all(copies, axis, split_axis=0, concat_axis=0, tiled=True)  25.7 us
    all_to_all x1, waiting for transfers between devices, on_device(): lax.all_to_all(spread[0], 'fs', split_axis=1, concat_axis=0, tiled=True)  22.3 us
    all_to_all x2, waiting for transfers between devices, copy_for_each(): return lax.all_to_all(copies, axis, split_axis=0, concat_axis=0, tiled=True)  18.6 us
  transfers between devices with their start and end apart: 6, of which 5 were waited for; matrix products, arithmetic and copies ran while one was open for 1% of the time, Pallas kernels for 0%

commit v1 on v0

v1 whole, which is shorter than its diff:
```python
import functools

import jax
import jax.numpy as jnp
from jax import lax
from jax.experimental import pallas as pl
from jax.experimental.pallas import tpu as pltpu
from jax.sharding import PartitionSpec as P

EPS = 1e-06
CORES = 2
MESH = pl.DeviceIdType.MESH


def rcopy(src, dst, send_sem, recv_sem, **where):
    return pltpu.make_async_remote_copy(
        src_ref=src, dst_ref=dst, send_sem=send_sem, recv_sem=recv_sem,
        device_id=where, device_id_type=MESH,
    )


def wait_bytes(ref, sem):
    pltpu.make_async_copy(ref, ref, sem).wait()


def kernel(
    Z, T,
    prompt, folded, downs,
    result, sg1, su1, sd1, sg2, su2, sd2,
    A, B, C, DN, NX, part, RL, RR, SL, SR, N,
    a_send, a_recv, b_send, b_recv, c_send, c_recv, p_recv, d_send, d_recv,
    rl_send, rl_recv, rr_send, rr_recv, gr_send, gr_recv, gl_send, gl_recv,
    loc, out_sem,
):
    z = lax.axis_index("fs")
    t = lax.axis_index("tp")
    X = T // CORES
    x, c = t // CORES, t % CORES
    H = Z // 2
    mats, rows, width = folded.shape
    rq = rows // X
    hid = DN.shape[1]
    zper = width // hid
    dcol = downs.shape[2]
    tok, D = NX.shape
    own = tok // Z
    half = D // 2
    right, left = lax.rem(z + 1, Z), lax.rem(z + Z - 1, Z)
    partner = t + 1 - 2 * c

    barrier = pltpu.get_barrier_semaphore()

    @pl.loop(1, Z)
    def _(k):
        pl.semaphore_signal(barrier, inc=1, device_id={"fs": lax.rem(z + k, Z)}, device_id_type=MESH)

    @pl.loop(1, T)
    def _(k):
        pl.semaphore_signal(barrier, inc=1, device_id={"tp": lax.rem(t + k, T)}, device_id_type=MESH)

    pl.semaphore_wait(barrier, Z + T - 2)

    def slice_of(layer, tt):
        return folded.at[2 * layer + tt // X, pl.ds(pl.multiple_of(lax.rem(tt, X) * rq, rq), rq), :]

    for layer in range(2):
        @pl.loop(1, T)
        def _(k):
            tt = lax.rem(t + k, T)
            rcopy(slice_of(layer, tt), A.at[layer, t], a_send.at[layer], a_recv.at[layer], tp=tt).start()

        pltpu.make_async_copy(slice_of(layer, t), A.at[layer, t], a_recv.at[layer]).start()

    for layer in range(2):
        mine = DN.at[layer, :, pl.ds(pl.multiple_of(t * dcol, dcol), dcol)]

        @pl.loop(1, T)
        def _(k):
            tt = lax.rem(t + k, T)
            rcopy(downs.at[layer], mine, d_send.at[layer], d_recv.at[layer], tp=tt).start()

        pltpu.make_async_copy(downs.at[layer], mine, d_recv.at[layer]).start()

    @pl.loop(0, tok // 16)
    def _(i):
        r = pl.ds(pl.multiple_of(i * 16, 16), 16)
        v = prompt[r, :].astype(jnp.float32)
        NX[r, :] = (v * lax.rsqrt(jnp.mean(v * v, axis=-1, keepdims=True) + EPS)).astype(jnp.bfloat16)

    pair = prompt[pl.ds(pl.multiple_of((z // 2) * 16, 16), 16), :].astype(jnp.float32)
    stream = jnp.where(lax.rem(z, 2) == 0, pair[:own], pair[own:])
    stream = jnp.concatenate([stream[:, :half], stream[:, half:]], axis=0)

    def block_for(layer, zz):
        return A.at[layer, zz // zper, :, pl.ds(pl.multiple_of(lax.rem(zz, zper) * hid, hid), hid)]

    def spread(layer, k):
        @pl.when(k < H)
        def _():
            zz = lax.rem(z + Z - k, Z)
            rcopy(block_for(layer, zz), B.at[layer, z], b_send.at[layer], b_recv.at[layer], fs=zz).start()

        zz = lax.rem(z + k, Z)
        rcopy(block_for(layer, zz), B.at[layer, z], b_send.at[layer], b_recv.at[layer], fs=zz).start()

    def spread_own(layer):
        pltpu.make_async_copy(block_for(layer, z), B.at[layer, z], b_recv.at[layer]).start()

    def rows_of(layer, tt):
        return C.at[2 * layer + tt // X, :, lax.rem(tt, X)]

    def gather_start(layer):
        wait_bytes(B.at[layer], b_recv.at[layer])
        for k in range(1, X):
            tt = lax.rem(t + CORES * k, T)
            rcopy(B.at[layer], rows_of(layer, t), c_send.at[layer], c_recv.at[layer, k - 1], tp=tt).start()
        rcopy(B.at[layer], rows_of(layer, t), c_send.at[layer], p_recv.at[layer], tp=partner).start()
        pltpu.make_async_copy(B.at[layer], rows_of(layer, t), loc.at[layer]).start()

    def gather_pass(layer):
        for k in (1, 3, 2) if X == 4 else range(1, X):
            tt = lax.rem(t + T - CORES * k, T)
            pltpu.make_async_copy(rows_of(layer, tt), rows_of(layer, tt), c_recv.at[layer, k - 1]).wait()
            rcopy(rows_of(layer, tt), rows_of(layer, tt), c_send.at[layer], p_recv.at[layer], tp=partner).start()

    def gather_end(layer):
        wait_bytes(C.at[2 * layer], p_recv.at[layer])
        pltpu.make_async_copy(B.at[layer], B.at[layer], loc.at[layer]).wait()
        for m, out in enumerate(((sg1, su1), (sg2, su2))[layer]):
            pltpu.make_async_copy(C.at[2 * layer + m], out, out_sem.at[2 * layer + m]).start()

    def partial_sums(layer):
        normed = NX[...]
        gate = jnp.dot(normed, C[2 * layer].reshape(D, hid), preferred_element_type=jnp.float32)
        up = jnp.dot(normed, C[2 * layer + 1].reshape(D, hid), preferred_element_type=jnp.float32)
        hidden = (gate / (1.0 + jnp.exp(-gate)) * up).astype(jnp.bfloat16)
        wait_bytes(DN.at[layer], d_recv.at[layer])
        pltpu.make_async_copy(DN.at[layer], (sd1, sd2)[layer], out_sem.at[4 + layer]).start()
        for h in range(2):
            got = jnp.dot(hidden, DN[layer, :, h * half:(h + 1) * half], preferred_element_type=jnp.float32)
            part[:, h * own:(h + 1) * own, :] = got.reshape(Z, own, half)

    def reduce_scatter(layer, beside):
        def step(s, first):
            dl = lax.rem(z + Z - H + s, Z)
            to_left = part[dl]
            if not first:
                pltpu.make_async_copy(RL.at[layer, s - 1], RL.at[layer, s - 1], rl_recv.at[layer, s - 1]).wait()
                to_left = to_left + RL[layer, s - 1].astype(jnp.float32)
            SL[layer, s] = to_left.astype(jnp.bfloat16)
            rcopy(SL.at[layer, s], RL.at[layer, s], rl_send.at[layer], rl_recv.at[layer, s], fs=left).start()

            def go_right():
                dr = lax.rem(z + H - 1 - s, Z)
                to_right = part[dr]
                if not first:
                    pltpu.make_async_copy(RR.at[layer, s - 1], RR.at[layer, s - 1], rr_recv.at[layer, s - 1]).wait()
                    to_right = to_right + RR[layer, s - 1].astype(jnp.float32)
                SR[layer, s] = to_right.astype(jnp.bfloat16)
                rcopy(SR.at[layer, s], RR.at[layer, s], rr_send.at[layer], rr_recv.at[layer, s], fs=right).start()

            if first:
                go_right()
            else:
                pl.when(s < H - 1)(go_right)
            beside(s)

        step(0, True)

        @pl.loop(1, H)
        def _(s):
            step(s, False)

        pltpu.make_async_copy(RR.at[layer, H - 2], RR.at[layer, H - 2], rr_recv.at[layer, H - 2]).wait()
        pltpu.make_async_copy(RL.at[layer, H - 1], RL.at[layer, H - 1], rl_recv.at[layer, H - 1]).wait()
        return part[z] + RR[layer, H - 2].astype(jnp.float32) + RL[layer, H - 1].astype(jnp.float32)

    def all_gather(layer, s0, s1):
        def step(s, first):
            ro = lax.rem(z + Z - s, Z)
            if not first:
                pltpu.make_async_copy(N.at[layer, ro], N.at[layer, ro], gr_recv.at[layer, s - 1]).wait()
            rcopy(N.at[layer, ro], N.at[layer, ro], gr_send.at[layer], gr_recv.at[layer, s], fs=right).start()

            def go_left():
                lo = lax.rem(z + s, Z)
                if not first:
                    pltpu.make_async_copy(N.at[layer, lo], N.at[layer, lo], gl_recv.at[layer, s - 1]).wait()
                rcopy(N.at[layer, lo], N.at[layer, lo], gl_send.at[layer], gl_recv.at[layer, s], fs=left).start()

            if first:
                go_left()
            else:
                pl.when(s < H - 1)(go_left)

        if s0 == 0:
            step(0, True)

        @pl.loop(max(s0, 1), s1)
        def _(s):
            step(s, False)

        if s1 == H:
            lo, ro = lax.rem(z + H - 1, Z), lax.rem(z + Z - H, Z)
            pltpu.make_async_copy(N.at[layer, lo], N.at[layer, lo], gl_recv.at[layer, H - 2]).wait()
            pltpu.make_async_copy(N.at[layer, ro], N.at[layer, ro], gr_recv.at[layer, H - 1]).wait()

    def in_rows(layer, out):
        @pl.loop(0, Z // 2)
        def _(i):
            a = N[layer, 2 * i].astype(jnp.float32)
            b = N[layer, 2 * i + 1].astype(jnp.float32)
            r = pl.ds(pl.multiple_of(i * 16, 16), 16)
            out[r, :half] = jnp.concatenate([a[:own], b[:own]], axis=0).astype(jnp.bfloat16)
            out[r, half:] = jnp.concatenate([a[own:], b[own:]], axis=0).astype(jnp.bfloat16)

    wait_bytes(A.at[0], a_recv.at[0])
    spread_own(0)

    @pl.loop(0, H)
    def _(i):
        spread(0, H - i)

    gather_start(0)
    gather_pass(0)
    gather_end(0)
    partial_sums(0)

    wait_bytes(A.at[1], a_recv.at[1])
    spread_own(1)
    total = reduce_scatter(0, lambda s: spread(1, s + 1))
    stream = stream + 0.5 * total
    mean = jnp.sum(stream * stream, axis=-1, keepdims=True)
    mean = (mean[:own] + mean[own:]) / D
    mean = jnp.concatenate([mean, mean], axis=0)
    N[0, z] = (stream * lax.rsqrt(mean + EPS)).astype(jnp.bfloat16)
    gather_start(1)
    mid = (H * 5) // 8
    all_gather(0, 0, mid)
    gather_pass(1)
    all_gather(0, mid, H)
    in_rows(0, NX)
    gather_end(1)
    partial_sums(1)
    total = reduce_scatter(1, lambda s: None)
    stream = stream + 0.5 * total
    N[1, z] = stream.astype(jnp.bfloat16)
    all_gather(1, 0, H)
    in_rows(1, NX)
    pltpu.make_async_copy(NX, result, out_sem.at[6]).start()

    for layer in range(2):
        wait_bytes(A.at[layer, pl.ds(0, T - 1)], a_send.at[layer])
        wait_bytes(B.at[layer, pl.ds(0, Z - 1)], b_send.at[layer])
        wait_bytes(C.at[2 * layer], c_send.at[layer])
        wait_bytes(C.at[2 * layer, :, pl.ds(0, X - 1)], c_send.at[layer])
        wait_bytes(DN.at[layer, :, pl.ds(0, (T - 1) * dcol)], d_send.at[layer])
        wait_bytes(SL.at[layer], rl_send.at[layer])
        wait_bytes(SR.at[layer, pl.ds(0, H - 1)], rr_send.at[layer])
        wait_bytes(N.at[layer, pl.ds(0, H)], gr_send.at[layer])
        wait_bytes(N.at[layer, pl.ds(0, H - 1)], gl_send.at[layer])
    for k, (src, dst) in enumerate(
        ((C.at[0], sg1), (C.at[1], su1), (C.at[2], sg2), (C.at[3], su2), (DN.at[0], sd1), (DN.at[1], sd2), (NX, result))
    ):
        pltpu.make_async_copy(src, dst, out_sem.at[k]).wait()


def fold(gain, weight):
    return (gain[:, None] * weight).astype(jnp.bfloat16)


def on_device(Z, T, prompt, g1, wg1, wu1, wd1, g2, wg2, wu2, wd2):
    bf = jnp.bfloat16
    folded = jnp.stack([fold(g1, wg1), fold(g1, wu1), fold(g2, wg2), fold(g2, wu2)])
    downs = jnp.stack([wd1.astype(bf), wd2.astype(bf)])
    X = T // CORES
    H = Z // 2
    rows, width = wg1.shape
    hid = wd1.shape[0]
    tok, D = prompt.shape
    own = tok // Z
    rq = rows // X
    served = jax.ShapeDtypeStruct((Z, X, rq, hid), bf)
    down = jax.ShapeDtypeStruct((hid, D), bf)
    dma = pltpu.SemaphoreType.DMA
    ring = (2, H, 2 * own, D // 2)
    outs = pl.pallas_call(
        functools.partial(kernel, Z, T),
        out_shape=(jax.ShapeDtypeStruct((tok, D), bf), served, served, down, served, served, down),
        in_specs=[pl.BlockSpec(memory_space=pltpu.VMEM)] * 3,
        out_specs=(pl.BlockSpec(memory_space=pl.ANY),) * 7,
        scratch_shapes=[
            pltpu.VMEM((2, T, rq, width), bf),
            pltpu.VMEM((2, Z, rq, hid), bf),
            pltpu.VMEM((4, Z, X, rq, hid), bf),
            pltpu.VMEM((2, hid, D), bf),
            pltpu.VMEM((tok, D), bf),
            pltpu.VMEM((Z, 2 * own, D // 2), jnp.float32),
            pltpu.VMEM(ring, bf), pltpu.VMEM(ring, bf), pltpu.VMEM(ring, bf), pltpu.VMEM(ring, bf),
            pltpu.VMEM((2, Z, 2 * own, D // 2), bf),
            dma((2,)), dma((2,)), dma((2,)), dma((2,)), dma((2,)), dma((2, X - 1)), dma((2,)), dma((2,)), dma((2,)),
            dma((2,)), dma((2, H)), dma((2,)), dma((2, H)), dma((2,)), dma((2, H)), dma((2,)), dma((2, H)),
            dma((2,)), dma((7,)),
        ],
        compiler_params=pltpu.CompilerParams(collective_id=0, has_side_effects=True),
        name="handoff",
    )(prompt, folded, downs)
    flat = lambda a: a.reshape(-1, hid)
    return (outs[0], flat(outs[1]), flat(outs[2]), outs[3], flat(outs[4]), flat(outs[5]), outs[6])


def solution(mesh):
    return jax.shard_map(
        functools.partial(on_device, mesh.shape["fs"], mesh.shape["tp"]),
        mesh=mesh,
        in_specs=(
            P(("grp", "tp"), None),
            P("fs"),
            P("fs", "tp"),
            P("fs", "tp"),
            P("fs", "tp"),
            P("fs"),
            P("fs", "tp"),
            P("fs", "tp"),
            P("fs", "tp"),
        ),
        out_specs=(
            P(("grp", "tp"), None),
            P("grp", "fs"),
            P("grp", "fs"),
            P("fs", "grp"),
            P("grp", "fs"),
            P("grp", "fs"),
            P("fs", "grp"),
        ),
        check_vma=False,
    )
```

time: 691 us -> 310 us (0.45)
  waiting for transfers between devices: 450 us -> 0 us
  Pallas kernels: 0 us -> 297 us
  blocking collectives: 147 us -> 0 us
  starting transfers between devices: 53.4 us -> 0 us
  between operations: 13.9 us -> 0.72 us
  other arithmetic: 9.56 us -> 2.54 us
    psum x2 -> x0, waiting for transfers between devices: 409 us -> none  [on_device(): stream = stream + 0.5 * lax.psum(partial_out, 'fs')]
    pallas_call x0 -> x1, Pallas kernels: none -> 297 us  [on_device(): pl.pallas_call(functools.partial(kernel, Z, T), out_shape=(jax.ShapeDtype...]
    all_to_all x9 -> x0, blocking collectives: 147 us -> none  [the longest x1 29.9 us: on_device(): lax.all_to_all(spread[2], 'fs', split_axis=1, concat_axis=0, tiled=True)]
    all_to_all x3 -> x0, starting transfers between devices: 53.2 us -> none  [the longest x1 45.8 us: on_device(): lax.all_to_all(spread[0], 'fs', split_axis=1, concat_axis=0, tiled=True)]
    all_to_all x3 -> x0, waiting for transfers between devices: 41 us -> none  [the longest x1 22.3 us: on_device(): lax.all_to_all(spread[0], 'fs', split_axis=1, concat_axis=0, tiled=True)]
    unnamed x20 -> x31, local copies, waits for them, and re-layouts: 2.73 us -> 9.64 us
  transfers between devices with their start and end apart: 6 -> 0, of which waited for: 5 -> 0; matrix products, arithmetic and copies ran while one was open for 1% -> 0% of each run, Pallas kernels for 0% -> 0%
where the time goes in v1:
time: 310 us
  Pallas kernels  297 us (96%)
  local copies, waits for them, and re-layouts  9.64 us (3%)
    pallas_call x1, Pallas kernels, on_device(): pl.pallas_call(functools.partial(kernel, Z, T), out_shape=(jax.ShapeDtype...  297 us
    unnamed x31, local copies, waits for them, and re-layouts  9.64 us

profile of v1, /device:TPU:40, one launch (start us, length us, event | category | flops | bytes accessed | tf_op | source)
XLA Modules:
  0.0 309.9 jit_solution(14371794468200938603)
XLA Ops:
  0.6 0.0 copy-start.8
  0.6 0.0 copy-start.9
  0.7 0.0 copy-start.10
  0.7 0.0 copy-start.11
  0.7 1.0 convert_bitcast_fusion
  1.7 0.0 copy-start.6
  1.7 0.0 copy-start.7
  1.7 0.7 pad_maximum_fusion.1.downs
  2.4 0.0 copy-done.8
  2.4 0.0 copy-done.9
  2.4 0.0 copy-done.10
  2.4 0.0 copy-done.11
  2.4 0.2 copy-done.6
  2.6 0.1 copy-done.7
  2.7 0.1 fusion
  2.8 0.7 pad_maximum_fusion.folded
  3.6 297.0 %handoff.1 = (bf16[256,2048]{1,0:T(8,128)(2,1)}, bf16[32,4,16,128]{3,2,1,0:T(8,128)(2,1)}, bf16[32,4,16,128]{3,2,1,0:T(8,128)(2,1)}, bf16[128,2048]{1,0:T(8,128)...) custom-call(bf16[256,2048]{1,0:T(8,128)(2,1)} %prompt.1, ...), custom_call_target="tpu_custom_call" | custom-call | tf_op jit(solution)/shard_map/handoff/pallas_call | solution.py:287
  300.6 0.0 copy-start.5
  300.6 2.4 copy.23
  303.0 0.0 copy-done.5
  303.0 0.0 copy-start.4
  303.0 0.8 copy.24
  303.8 0.4 copy-done.4
  304.2 0.0 copy-start.3
  304.2 0.8 copy.25
  305.0 0.4 copy-done.3
  305.4 0.0 copy-start.2
  305.4 0.8 copy.26
  306.2 0.4 copy-done.2
  306.7 0.0 copy-start.1
  306.7 0.8 copy.27
  307.5 0.4 copy-done.1
  307.9 0.0 copy-start
  307.9 0.8 copy.28
  308.7 0.4 copy-done
  309.1 0.8 copy.29
Async XLA Ops:
  0.6 1.8 copy-start.8
  0.6 1.8 copy-start.9
  0.7 1.8 copy-start.10
  0.7 1.8 copy-start.11
  1.7 0.9 copy-start.6
  1.7 1.0 copy-start.7
  300.6 2.4 copy-start.5
  303.0 1.2 copy-start.4
  304.2 1.2 copy-start.3
  305.4 1.2 copy-start.2
  306.7 1.2 copy-start.1
  307.9 1.2 copy-start

commit v2 on v1

--- a/solution.py
+++ b/solution.py
@@ -10,6 +10,7 @@
 EPS = 1e-06
 CORES = 2
 MESH = pl.DeviceIdType.MESH
+HOPS = (2, 4, 4, 4)
 
 
 def rcopy(src, dst, send_sem, recv_sem, **where):
@@ -27,9 +28,9 @@
     Z, T,
     prompt, folded, downs,
     result, sg1, su1, sd1, sg2, su2, sd2,
-    A, B, C, DN, NX, part, RL, RR, SL, SR, N,
+    A, B, C, DN, NX, part, R, S, N,
     a_send, a_recv, b_send, b_recv, c_send, c_recv, p_recv, d_send, d_recv,
-    rl_send, rl_recv, rr_send, rr_recv, gr_send, gr_recv, gl_send, gl_recv,
+    r_send, r_recv, g_send, g_recv,
     loc, out_sem,
 ):
     z = lax.axis_index("fs")
@@ -45,7 +46,6 @@
     tok, D = NX.shape
     own = tok // Z
     half = D // 2
-    right, left = lax.rem(z + 1, Z), lax.rem(z + Z - 1, Z)
     partner = t + 1 - 2 * c
 
     barrier = pltpu.get_barrier_semaphore()
@@ -140,70 +140,106 @@
             got = jnp.dot(hidden, DN[layer, :, h * half:(h + 1) * half], preferred_element_type=jnp.float32)
             part[:, h * own:(h + 1) * own, :] = got.reshape(Z, own, half)
 
-    def reduce_scatter(layer, beside):
-        def step(s, first):
-            dl = lax.rem(z + Z - H + s, Z)
-            to_left = part[dl]
-            if not first:
-                pltpu.make_async_copy(RL.at[layer, s - 1], RL.at[layer, s - 1], rl_recv.at[layer, s - 1]).wait()
-                to_left = to_left + RL[layer, s - 1].astype(jnp.float32)
-            SL[layer, s] = to_left.astype(jnp.bfloat16)
-            rcopy(SL.at[layer, s], RL.at[layer, s], rl_send.at[layer], rl_recv.at[layer, s], fs=left).start()
-
-            def go_right():
-                dr = lax.rem(z + H - 1 - s, Z)
-                to_right = part[dr]
-                if not first:
-                    pltpu.make_async_copy(RR.at[layer, s - 1], RR.at[layer, s - 1], rr_recv.at[layer, s - 1]).wait()
-                    to_right = to_right + RR[layer, s - 1].astype(jnp.float32)
-                SR[layer, s] = to_right.astype(jnp.bfloat16)
-                rcopy(SR.at[layer, s], RR.at[layer, s], rr_send.at[layer], rr_recv.at[layer, s], fs=right).start()
-
-            if first:
-                go_right()
-            else:
-                pl.when(s < H - 1)(go_right)
+    reach = (H, H - 1)
+
+    def at(side, m):
+        return lax.rem(z + (Z - m if side == 0 else m), Z)
+
+    def reduce_scatter(layer, K, beside):
+        def send(side, m, i):
+            rcopy(
+                S.at[layer, side, m - 1], R.at[layer, side, m - 1],
+                r_send.at[layer, side], r_recv.at[layer, side, m - 1], fs=at(side, i),
+            ).start()
+
+        def arrived(side, m):
+            slot = R.at[layer, side, m - 1]
+            pltpu.make_async_copy(slot, slot, r_recv.at[layer, side, m - 1]).wait()
+            return R[layer, side, m - 1].astype(jnp.float32)
+
+        def raws(side, g, static=True):
+            for i in range(K, 0, -1):
+                m = g * K + i
+                if static and m > reach[side]:
+                    continue
+                if i == K and not (static and m + 1 > reach[side]):
+                    continue
+                S[layer, side, m - 1] = part[at(side, m)].astype(jnp.bfloat16)
+                send(side, m, i)
+
+        def node(side, j, static=True):
+            acc = part[at(side, j * K)]
+            for i in range(1, K + 1):
+                if static and j * K + i > reach[side]:
+                    continue
+                acc = acc + arrived(side, j * K + i)
+            S[layer, side, j * K - 1] = acc.astype(jnp.bfloat16)
+            send(side, j * K, K)
+
+        steps = [-(-M // K) for M in reach]
+        low = min(steps) - 1
+        for side in range(2):
+            raws(side, steps[side] - 1)
+        for j in range(max(steps) - 1, max(low, 1) - 1, -1):
+            for side in range(2):
+                if j < steps[side]:
+                    node(side, j)
+                    raws(side, j - 1)
+        beside(0)
+
+        @pl.loop(1, low)
+        def _(s):
+            for side in range(2):
+                node(side, low - s, False)
+                raws(side, low - s - 1, False)
             beside(s)
 
-        step(0, True)
-
-        @pl.loop(1, H)
+        total = part[z]
+        for i in range(1, K + 1):
+            for side in range(2):
+                total = total + arrived(side, i)
+        return total
+
+    span = (H - 1, H)
+
+    def all_gather(layer, K, beside):
+        def arrived(side, m):
+            slot = N.at[layer, at(side, m)]
+            pltpu.make_async_copy(slot, slot, g_recv.at[layer, side, m - 1]).wait()
+
+        def step(side, s, static=True):
+            for h in range(K, 0, -1):
+                if static and s * K + h > span[side]:
+                    continue
+                slot = N.at[layer, at(side, s * K)]
+                rcopy(
+                    slot, slot, g_send.at[layer, side], g_recv.at[layer, side, s * K + h - 1],
+                    fs=at(1 - side, h),
+                ).start()
+
+        steps = [-(-M // K) for M in span]
+        low = min(steps) - 1
+        for side in range(2):
+            step(side, 0)
+
+        @pl.loop(1, low)
         def _(s):
-            step(s, False)
-
-        pltpu.make_async_copy(RR.at[layer, H - 2], RR.at[layer, H - 2], rr_recv.at[layer, H - 2]).wait()
-        pltpu.make_async_copy(RL.at[layer, H - 1], RL.at[layer, H - 1], rl_recv.at[layer, H - 1]).wait()
-        return part[z] + RR[layer, H - 2].astype(jnp.float32) + RL[layer, H - 1].astype(jnp.float32)
-
-    def all_gather(layer, s0, s1):
-        def step(s, first):
-            ro = lax.rem(z + Z - s, Z)
-            if not first:
-                pltpu.make_async_copy(N.at[layer, ro], N.at[layer, ro], gr_recv.at[layer, s - 1]).wait()
-            rcopy(N.at[layer, ro], N.at[layer, ro], gr_send.at[layer], gr_recv.at[layer, s], fs=right).start()
-
-            def go_left():
-                lo = lax.rem(z + s, Z)
-                if not first:
-                    pltpu.make_async_copy(N.at[layer, lo], N.at[layer, lo], gl_recv.at[layer, s - 1]).wait()
-                rcopy(N.at[layer, lo], N.at[layer, lo], gl_send.at[layer], gl_recv.at[layer, s], fs=left).start()
-
-            if first:
-                go_left()
-            else:
-                pl.when(s < H - 1)(go_left)
-
-        if s0 == 0:
-            step(0, True)
-
-        @pl.loop(max(s0, 1), s1)
-        def _(s):
-            step(s, False)
-
-        if s1 == H:
-            lo, ro = lax.rem(z + H - 1, Z), lax.rem(z + Z - H, Z)
-            pltpu.make_async_copy(N.at[layer, lo], N.at[layer, lo], gl_recv.at[layer, H - 2]).wait()
-            pltpu.make_async_copy(N.at[layer, ro], N.at[layer, ro], gr_recv.at[layer, H - 1]).wait()
+            for side in range(2):
+                arrived(side, s * K)
+                step(side, s, False)
+
+        for s in range(max(low, 1), max(steps)):
+            for side in range(2):
+                if s < steps[side]:
+                    arrived(side, s * K)
+                    step(side, s)
+        beside()
+        for side in range(2):
+            for g in range(steps[side]):
+                for i in range(1, K + 1):
+                    m = g * K + i
+                    if m <= span[side] and not (i == K and g < steps[side] - 1):
+                        arrived(side, m)
 
     def in_rows(layer, out):
         @pl.loop(0, Z // 2)
@@ -228,24 +264,29 @@
 
     wait_bytes(A.at[1], a_recv.at[1])
     spread_own(1)
-    total = reduce_scatter(0, lambda s: spread(1, s + 1))
+    K = HOPS[0]
+    rounds = max(-(-(H - 1) // K) - 1, 1)
+
+    def spread_some(s):
+        for i in range(-(-H // rounds)):
+            k = H - s * -(-H // rounds) - i
+            pl.when(k > 0)(lambda: spread(1, k))
+
+    total = reduce_scatter(0, K, spread_some)
     stream = stream + 0.5 * total
     mean = jnp.sum(stream * stream, axis=-1, keepdims=True)
     mean = (mean[:own] + mean[own:]) / D
     mean = jnp.concatenate([mean, mean], axis=0)
     N[0, z] = (stream * lax.rsqrt(mean + EPS)).astype(jnp.bfloat16)
     gather_start(1)
-    mid = (H * 5) // 8
-    all_gather(0, 0, mid)
-    gather_pass(1)
-    all_gather(0, mid, H)
+    all_gather(0, HOPS[1], lambda: gather_pass(1))
     in_rows(0, NX)
     gather_end(1)
     partial_sums(1)
-    total = reduce_scatter(1, lambda s: None)
+    total = reduce_scatter(1, HOPS[2], lambda s: None)
     stream = stream + 0.5 * total
     N[1, z] = stream.astype(jnp.bfloat16)
-    all_gather(1, 0, H)
+    all_gather(1, HOPS[3], lambda: None)
     in_rows(1, NX)
     pltpu.make_async_copy(NX, result, out_sem.at[6]).start()
 
@@ -255,10 +296,9 @@
         wait_bytes(C.at[2 * layer], c_send.at[layer])
         wait_bytes(C.at[2 * layer, :, pl.ds(0, X - 1)], c_send.at[layer])
         wait_bytes(DN.at[layer, :, pl.ds(0, (T - 1) * dcol)], d_send.at[layer])
-        wait_bytes(SL.at[layer], rl_send.at[layer])
-        wait_bytes(SR.at[layer, pl.ds(0, H - 1)], rr_send.at[layer])
-        wait_bytes(N.at[layer, pl.ds(0, H)], gr_send.at[layer])
-        wait_bytes(N.at[layer, pl.ds(0, H - 1)], gl_send.at[layer])
+        for side in range(2):
+            wait_bytes(S.at[layer, side, pl.ds(0, reach[side])], r_send.at[layer, side])
+            wait_bytes(N.at[layer, pl.ds(0, span[side])], g_send.at[layer, side])
     for k, (src, dst) in enumerate(
         ((C.at[0], sg1), (C.at[1], su1), (C.at[2], sg2), (C.at[3], su2), (DN.at[0], sd1), (DN.at[1], sd2), (NX, result))
     ):
@@ -283,7 +323,7 @@
     served = jax.ShapeDtypeStruct((Z, X, rq, hid), bf)
     down = jax.ShapeDtypeStruct((hid, D), bf)
     dma = pltpu.SemaphoreType.DMA
-    ring = (2, H, 2 * own, D // 2)
+    ring = (2, 2, H, 2 * own, D // 2)
     outs = pl.pallas_call(
         functools.partial(kernel, Z, T),
         out_shape=(jax.ShapeDtypeStruct((tok, D), bf), served, served, down, served, served, down),
@@ -296,10 +336,10 @@
             pltpu.VMEM((2, hid, D), bf),
             pltpu.VMEM((tok, D), bf),
             pltpu.VMEM((Z, 2 * own, D // 2), jnp.float32),
-            pltpu.VMEM(ring, bf), pltpu.VMEM(ring, bf), pltpu.VMEM(ring, bf), pltpu.VMEM(ring, bf),
+            pltpu.VMEM(ring, bf), pltpu.VMEM(ring, bf),
             pltpu.VMEM((2, Z, 2 * own, D // 2), bf),
             dma((2,)), dma((2,)), dma((2,)), dma((2,)), dma((2,)), dma((2, X - 1)), dma((2,)), dma((2,)), dma((2,)),
-            dma((2,)), dma((2, H)), dma((2,)), dma((2, H)), dma((2,)), dma((2, H)), dma((2,)), dma((2, H)),
+            dma((2, 2)), dma((2, 2, H)), dma((2, 2)), dma((2, 2, H)),
             dma((2,)), dma((7,)),
         ],
         compiler_params=pltpu.CompilerParams(collective_id=0, has_side_effects=True),

time: 310 us -> 238 us (0.77)
  Pallas kernels: 297 us -> 225 us
    pallas_call x1, Pallas kernels: 297 us -> 225 us  [on_device(): pl.pallas_call(functools.partial(kernel, Z, T), out_shape=(jax.ShapeDtype...]
where the time goes in v2:
time: 238 us
  Pallas kernels  225 us (95%)
  local copies, waits for them, and re-layouts  9.64 us (4%)
  other arithmetic  2.54 us (1%)
    pallas_call x1, Pallas kernels, on_device(): pl.pallas_call(functools.partial(kernel, Z, T), out_shape=(jax.ShapeDtype...  225 us
    unnamed x31, local copies, waits for them, and re-layouts  9.64 us

profile of v2, /device:TPU:40, one launch (start us, length us, event | category | flops | bytes accessed | tf_op | source)
XLA Modules:
  0.0 238.0 jit_solution(4231353593855858862)
XLA Ops:
  0.6 0.0 copy-start.8
  0.6 0.0 copy-start.9
  0.7 0.0 copy-start.10
  0.7 0.0 copy-start.11
  0.7 1.0 convert_bitcast_fusion
  1.7 0.0 copy-start.6
  1.7 0.0 copy-start.7
  1.7 0.7 pad_maximum_fusion.1.downs
  2.4 0.0 copy-done.8
  2.4 0.0 copy-done.9
  2.4 0.0 copy-done.10
  2.4 0.0 copy-done.11
  2.4 0.2 copy-done.6
  2.6 0.1 copy-done.7
  2.7 0.1 fusion
  2.8 0.7 pad_maximum_fusion.folded
  3.6 225.1 %handoff.1 = (bf16[256,2048]{1,0:T(8,128)(2,1)}, bf16[32,4,16,128]{3,2,1,0:T(8,128)(2,1)}, bf16[32,4,16,128]{3,2,1,0:T(8,128)(2,1)}, bf16[128,2048]{1,0:T(8,128)...) custom-call(bf16[256,2048]{1,0:T(8,128)(2,1)} %prompt.1, ...), custom_call_target="tpu_custom_call" | custom-call | tf_op jit(solution)/shard_map/handoff/pallas_call | solution.py:327
  228.6 0.0 copy-start.5
  228.7 2.4 copy.23
  231.0 0.0 copy-done.5
  231.0 0.0 copy-start.4
  231.0 0.8 copy.24
  231.8 0.4 copy-done.4
  232.2 0.0 copy-start.3
  232.2 0.8 copy.25
  233.0 0.4 copy-done.3
  233.5 0.0 copy-start.2
  233.5 0.8 copy.26
  234.3 0.4 copy-done.2
  234.7 0.0 copy-start.1
  234.7 0.8 copy.27
  235.5 0.4 copy-done.1
  235.9 0.0 copy-start
  235.9 0.8 copy.28
  236.7 0.4 copy-done
  237.2 0.8 copy.29
Async XLA Ops:
  0.6 1.8 copy-start.8
  0.6 1.8 copy-start.9
  0.7 1.8 copy-start.10
  0.7 1.8 copy-start.11
  1.7 0.9 copy-start.6
  1.7 1.0 copy-start.7
  228.6 2.4 copy-start.5
  231.0 1.2 copy-start.4
  232.2 1.2 copy-start.3
  233.5 1.2 copy-start.2
  234.7 1.2 copy-start.1
  235.9 1.2 copy-start

commit v3 on v2

v3 whole, which is shorter than its diff:
```python
import functools

import jax
import jax.numpy as jnp
from jax import lax
from jax.experimental import pallas as pl
from jax.experimental.pallas import tpu as pltpu
from jax.sharding import PartitionSpec as P

EPS = 1e-06
VMEM = 67_043_328
CORES = 2
MESH = pl.DeviceIdType.MESH
TREE = (0, 1, 0, 3, 4, 0)


def tree(span):
    K = len(TREE)
    parent = {m: (m - 1) // K * K + TREE[(m - 1) % K] for m in range(1, span + 1)}
    feeds = {a: [m for m in range(span, 0, -1) if parent[m] == a] for a in range(span + 1)}
    starts = [a for a in range(0, span + 1, K) if feeds[a]]
    order = []
    for k in range(len(starts) + 1):
        order += starts[k:k + 1]
        if k:
            order += [a for a in range(starts[k - 1] + 1, starts[k - 1] + K) if feeds.get(a)]
    return parent, feeds, order


def alternate(*lists):
    return [(side, step[k]) for k in range(max(map(len, lists))) for side, step in enumerate(lists) if k < len(step)]


def rcopy(src, dst, send_sem, recv_sem, **where):
    return pltpu.make_async_remote_copy(
        src_ref=src, dst_ref=dst, send_sem=send_sem, recv_sem=recv_sem,
        device_id=where, device_id_type=MESH,
    )


def wait_bytes(ref, sem):
    pltpu.make_async_copy(ref, ref, sem).wait()


def kernel(
    Z, T,
    prompt_in, g1, wg1, wu1, wd1, g2, wg2, wu2, wd2,
    C, DN, NX,
    prompt, gains, wide, tall, folded, downs,
    A, B, part, R, S, N,
    a_send, a_recv, b_send, b_recv, c_send, c_recv, p_recv, d_send, d_recv,
    r_send, r_recv, g_send, g_recv,
    loc, load_sem,
):
    z = lax.axis_index("fs")
    t = lax.axis_index("tp")
    X = T // CORES
    x, c = t // CORES, t % CORES
    H = Z // 2
    mats, rows, width = folded.shape
    rq = rows // X
    hid = DN.shape[1]
    zper = width // hid
    dcol = downs.shape[2]
    tok, D = NX.shape
    own = tok // Z
    half = D // 2
    partner = t + 1 - 2 * c

    loads = [(prompt_in, prompt)]
    for layer, (g, wg, wu, wd) in enumerate(((g1, wg1, wu1, wd1), (g2, wg2, wu2, wd2))):
        loads += [(g, gains.at[layer]), (wg, wide.at[2 * layer]), (wu, wide.at[2 * layer + 1]), (wd, tall.at[layer])]
    loads = [pltpu.make_async_copy(src, dst, load_sem.at[k]) for k, (src, dst) in enumerate(loads)]
    for k in (1, 2, 3, 5, 6, 7, 4, 8, 0):
        loads[k].start()

    barrier = pltpu.get_barrier_semaphore()

    @pl.loop(1, Z)
    def _(k):
        pl.semaphore_signal(barrier, inc=1, device_id={"fs": lax.rem(z + k, Z)}, device_id_type=MESH)

    @pl.loop(1, T)
    def _(k):
        pl.semaphore_signal(barrier, inc=1, device_id={"tp": lax.rem(t + k, T)}, device_id_type=MESH)

    for layer in range(2):
        for k in range(1, 4):
            loads[4 * layer + k].wait()
        diagonal = lax.broadcasted_iota(jnp.int32, (rows, rows), 0) == lax.broadcasted_iota(jnp.int32, (rows, rows), 1)
        gain = jnp.sum(jnp.where(diagonal, gains[layer], 0.0), axis=1, keepdims=True)
        for m in (2 * layer, 2 * layer + 1):
            folded[m] = (gain * wide[m]).astype(jnp.bfloat16)
    for layer in range(2):
        loads[4 * layer + 4].wait()
        downs[layer] = tall[layer].astype(jnp.bfloat16)
    loads[0].wait()

    @pl.loop(0, tok // 16)
    def _(i):
        r = pl.ds(pl.multiple_of(i * 16, 16), 16)
        v = prompt[r, :].astype(jnp.float32)
        NX[r, :] = (v * lax.rsqrt(jnp.mean(v * v, axis=-1, keepdims=True) + EPS)).astype(jnp.bfloat16)

    pair = prompt[pl.ds(pl.multiple_of((z // 2) * 16, 16), 16), :].astype(jnp.float32)
    stream = jnp.where(lax.rem(z, 2) == 0, pair[:own], pair[own:])
    stream = jnp.concatenate([stream[:, :half], stream[:, half:]], axis=0)

    pl.semaphore_wait(barrier, Z + T - 2)

    pend = {}

    def due(name, ref, sem):
        pend[name] = lambda: wait_bytes(ref, sem)

    def settle(name):
        pend.pop(name)()

    def finish():
        for name in list(pend):
            settle(name)

    def slice_of(layer, tt):
        return folded.at[2 * layer + tt // X, pl.ds(pl.multiple_of(lax.rem(tt, X) * rq, rq), rq), :]

    for layer in range(2):
        @pl.loop(1, T)
        def _(k):
            tt = lax.rem(t + k, T)
            rcopy(slice_of(layer, tt), A.at[layer, t], a_send.at[layer], a_recv.at[layer], tp=tt).start()

        pltpu.make_async_copy(slice_of(layer, t), A.at[layer, t], a_recv.at[layer]).start()
        due(f"A{layer}", A.at[layer], a_recv.at[layer])
        due(f"As{layer}", A.at[layer, pl.ds(0, T - 1)], a_send.at[layer])

    for layer in range(2):
        mine = DN.at[layer, :, pl.ds(pl.multiple_of(t * dcol, dcol), dcol)]

        @pl.loop(1, T)
        def _(k):
            tt = lax.rem(t + k, T)
            rcopy(downs.at[layer], mine, d_send.at[layer], d_recv.at[layer], tp=tt).start()

        pltpu.make_async_copy(downs.at[layer], mine, d_recv.at[layer]).start()
        due(f"D{layer}", DN.at[layer], d_recv.at[layer])
        due(f"Ds{layer}", DN.at[layer, :, pl.ds(0, (T - 1) * dcol)], d_send.at[layer])

    def block_for(layer, zz):
        return A.at[layer, zz // zper, :, pl.ds(pl.multiple_of(lax.rem(zz, zper) * hid, hid), hid)]

    def spread(layer, k):
        @pl.when(k < H)
        def _():
            zz = lax.rem(z + Z - k, Z)
            rcopy(block_for(layer, zz), B.at[layer, z], b_send.at[layer], b_recv.at[layer], fs=zz).start()

        zz = lax.rem(z + k, Z)
        rcopy(block_for(layer, zz), B.at[layer, z], b_send.at[layer], b_recv.at[layer], fs=zz).start()

    def spread_own(layer):
        pltpu.make_async_copy(block_for(layer, z), B.at[layer, z], b_recv.at[layer]).start()
        due(f"B{layer}", B.at[layer], b_recv.at[layer])
        due(f"Bs{layer}", B.at[layer, pl.ds(0, Z - 1)], b_send.at[layer])

    def rows_of(layer, tt):
        return C.at[2 * layer + tt // X, :, lax.rem(tt, X)]

    def gather_start(layer):
        settle(f"B{layer}")
        for k in range(1, X):
            tt = lax.rem(t + CORES * k, T)
            rcopy(B.at[layer], rows_of(layer, t), c_send.at[layer], c_recv.at[layer, k - 1], tp=tt).start()
        rcopy(B.at[layer], rows_of(layer, t), c_send.at[layer], p_recv.at[layer], tp=partner).start()
        pltpu.make_async_copy(B.at[layer], rows_of(layer, t), loc.at[layer]).start()
        due(f"Cp{layer}", C.at[2 * layer], p_recv.at[layer])
        due(f"Co{layer}", B.at[layer], loc.at[layer])
        due(f"Cs{layer}", C.at[2 * layer], c_send.at[layer])
        due(f"Ct{layer}", C.at[2 * layer, :, pl.ds(0, X - 1)], c_send.at[layer])

    def gather_pass(layer):
        for k in (1, 3, 2) if X == 4 else range(1, X):
            tt = lax.rem(t + T - CORES * k, T)
            pltpu.make_async_copy(rows_of(layer, tt), rows_of(layer, tt), c_recv.at[layer, k - 1]).wait()
            rcopy(rows_of(layer, tt), rows_of(layer, tt), c_send.at[layer], p_recv.at[layer], tp=partner).start()

    def gather_end(layer):
        settle(f"Cp{layer}")
        settle(f"Co{layer}")

    def partial_sums(layer):
        normed = NX[...]
        gate = jnp.dot(normed, C[2 * layer].reshape(D, hid), preferred_element_type=jnp.float32)
        up = jnp.dot(normed, C[2 * layer + 1].reshape(D, hid), preferred_element_type=jnp.float32)
        hidden = (gate / (1.0 + jnp.exp(-gate)) * up).astype(jnp.bfloat16)
        settle(f"D{layer}")
        for h in range(2):
            got = jnp.dot(hidden, DN[layer, :, h * half:(h + 1) * half], preferred_element_type=jnp.float32)
            part[:, h * own:(h + 1) * own, :] = got.reshape(Z, own, half)

    reach = (H, H - 1)

    def at(side, m):
        return lax.rem(z + (Z - m if side == 0 else m), Z)

    def reduce_scatter(layer):
        trees = [tree(M) for M in reach]

        def send(side, m, value):
            S[layer, side, m - 1] = value.astype(jnp.bfloat16)
            rcopy(
                S.at[layer, side, m - 1], R.at[layer, side, m - 1],
                r_send.at[layer, side], r_recv.at[layer, side, m - 1], fs=at(side, m - trees[side][0][m]),
            ).start()

        def gathered(side, a):
            acc = part[at(side, a)]
            for m in reversed(trees[side][1][a]):
                slot = R.at[layer, side, m - 1]
                pltpu.make_async_copy(slot, slot, r_recv.at[layer, side, m - 1]).wait()
                acc = acc + R[layer, side, m - 1].astype(jnp.float32)
            return acc

        def own_sums(side, k):
            _, feeds, order = trees[side]
            nodes = order[::-1]
            if k < len(nodes):
                for m in feeds[nodes[k]]:
                    if not feeds[m]:
                        send(side, m, part[at(side, m)])

        lead = 2
        for k in range(lead):
            for side in range(2):
                own_sums(side, k)
        for side, (k, a) in alternate(*([*enumerate(trees[i][2][::-1])] for i in range(2))):
            if a:
                send(side, a, gathered(side, a))
                own_sums(side, k + lead)
        for side in range(2):
            due(f"Rs{layer}{side}", S.at[layer, side, pl.ds(0, reach[side])], r_send.at[layer, side])
        return gathered(0, 0) + gathered(1, 0) - part[z]

    span = (H - 1, H)

    def all_gather(layer, beside):
        trees = [tree(M) for M in span]

        def arrived(side, m):
            slot = N.at[layer, at(side, m)]
            pltpu.make_async_copy(slot, slot, g_recv.at[layer, side, m - 1]).wait()

        for side, a in alternate(trees[0][2], trees[1][2]):
            if a:
                arrived(side, a)
            for m in trees[side][1][a]:
                slot = N.at[layer, at(side, a)]
                rcopy(
                    slot, slot, g_send.at[layer, side], g_recv.at[layer, side, m - 1], fs=at(1 - side, m - a),
                ).start()
        beside()
        for side in range(2):
            due(f"Gs{layer}{side}", N.at[layer, pl.ds(0, span[side])], g_send.at[layer, side])
            for m in range(1, span[side] + 1):
                if not trees[side][1][m]:
                    arrived(side, m)

    def in_rows(layer, out):
        @pl.loop(0, Z // 2)
        def _(i):
            a = N[layer, 2 * i].astype(jnp.float32)
            b = N[layer, 2 * i + 1].astype(jnp.float32)
            r = pl.ds(pl.multiple_of(i * 16, 16), 16)
            out[r, :half] = jnp.concatenate([a[:own], b[:own]], axis=0).astype(jnp.bfloat16)
            out[r, half:] = jnp.concatenate([a[own:], b[own:]], axis=0).astype(jnp.bfloat16)

    settle("A0")
    spread_own(0)

    @pl.loop(0, H)
    def _(i):
        spread(0, H - i)

    gather_start(0)
    settle("A1")
    spread_own(1)

    @pl.loop(0, H)
    def _(i):
        spread(1, H - i)

    gather_pass(0)
    gather_end(0)
    partial_sums(0)
    total = reduce_scatter(0)
    stream = stream + 0.5 * total
    mean = jnp.sum(stream * stream, axis=-1, keepdims=True)
    mean = (mean[:own] + mean[own:]) / D
    mean = jnp.concatenate([mean, mean], axis=0)
    N[0, z] = (stream * lax.rsqrt(mean + EPS)).astype(jnp.bfloat16)
    gather_start(1)
    all_gather(0, lambda: gather_pass(1))
    in_rows(0, NX)
    gather_end(1)
    partial_sums(1)
    total = reduce_scatter(1)
    stream = stream + 0.5 * total
    N[1, z] = stream.astype(jnp.bfloat16)
    all_gather(1, lambda: None)
    in_rows(1, NX)
    finish()


def put_out(C, DN, NX, result, sg1, su1, sd1, sg2, su2, sd2, sem):
    pairs = ((C.at[0], sg1), (C.at[1], su1), (C.at[2], sg2), (C.at[3], su2), (DN.at[0], sd1), (DN.at[1], sd2), (NX, result))
    copies = [pltpu.make_async_copy(src, dst, sem.at[k]) for k, (src, dst) in enumerate(pairs)]
    for copy in copies:
        copy.start()
    for copy in copies:
        copy.wait()


def on_device(Z, T, prompt, g1, wg1, wu1, wd1, g2, wg2, wu2, wd2):
    bf, f32 = jnp.bfloat16, jnp.float32
    X = T // CORES
    H = Z // 2
    rows, width = wg1.shape
    hid, dcol = wd1.shape
    tok, D = prompt.shape
    own = tok // Z
    rq = rows // X
    served = jax.ShapeDtypeStruct((Z, X, rq, hid), bf)
    down = jax.ShapeDtypeStruct((hid, D), bf)
    dma = pltpu.SemaphoreType.DMA
    ring = (2, 2, H, 2 * own, D // 2)
    anywhere = pl.BlockSpec(memory_space=pl.ANY)
    in_vmem = pl.BlockSpec(memory_space=pltpu.VMEM)
    held = pl.pallas_call(
        functools.partial(kernel, Z, T),
        out_shape=(pltpu.VMEM((4, Z, X, rq, hid), bf), pltpu.VMEM((2, hid, D), bf), pltpu.VMEM((tok, D), bf)),
        in_specs=[anywhere] * 9,
        out_specs=(in_vmem,) * 3,
        scratch_shapes=[
            pltpu.VMEM((tok, D), bf),
            pltpu.VMEM((2, 1, rows), f32),
            pltpu.VMEM((4, rows, width), f32),
            pltpu.VMEM((2, hid, dcol), f32),
            pltpu.VMEM((4, rows, width), bf),
            pltpu.VMEM((2, hid, dcol), bf),
            pltpu.VMEM((2, T, rq, width), bf),
            pltpu.VMEM((2, Z, rq, hid), bf),
            pltpu.VMEM((Z, 2 * own, D // 2), f32),
            pltpu.VMEM(ring, bf), pltpu.VMEM(ring, bf),
            pltpu.VMEM((2, Z, 2 * own, D // 2), bf),
            dma((2,)), dma((2,)), dma((2,)), dma((2,)), dma((2,)), dma((2, X - 1)), dma((2,)), dma((2,)), dma((2,)),
            dma((2, 2)), dma((2, 2, H)), dma((2, 2)), dma((2, 2, H)),
            dma((2,)), dma((9,)),
        ],
        compiler_params=pltpu.CompilerParams(collective_id=0, has_side_effects=True, vmem_limit_bytes=VMEM - 2 * (4 * Z * X * rq * hid + 2 * hid * D + tok * D)),
        name="handoff",
    )(prompt, g1.reshape(1, rows), wg1, wu1, wd1, g2.reshape(1, rows), wg2, wu2, wd2)
    outs = pl.pallas_call(
        put_out,
        out_shape=(jax.ShapeDtypeStruct((tok, D), bf), served, served, down, served, served, down),
        in_specs=[in_vmem] * 3,
        out_specs=(anywhere,) * 7,
        scratch_shapes=[dma((7,))],
        compiler_params=pltpu.CompilerParams(vmem_limit_bytes=8 * 2**20),
        name="put_out",
    )(*held)
    flat = lambda a: a.reshape(-1, hid)
    return (outs[0], flat(outs[1]), flat(outs[2]), outs[3], flat(outs[4]), flat(outs[5]), outs[6])


def solution(mesh):
    return jax.shard_map(
        functools.partial(on_device, mesh.shape["fs"], mesh.shape["tp"]),
        mesh=mesh,
        in_specs=(
            P(("grp", "tp"), None),
            P("fs"),
            P("fs", "tp"),
            P("fs", "tp"),
            P("fs", "tp"),
            P("fs"),
            P("fs", "tp"),
            P("fs", "tp"),
            P("fs", "tp"),
        ),
        out_specs=(
            P(("grp", "tp"), None),
            P("grp", "fs"),
            P("grp", "fs"),
            P("fs", "grp"),
            P("grp", "fs"),
            P("grp", "fs"),
            P("fs", "grp"),
        ),
        check_vma=False,
    )
```

time: 238 us -> 209 us (0.88)
  Pallas kernels: 225 us -> 207 us
  local copies, waits for them, and re-layouts: 9.64 us -> 0 us
  other arithmetic: 2.54 us -> 0 us
    pallas_call x1 -> x2, Pallas kernels: 225 us -> 207 us  [the longest x1 205 us: on_device(): pl.pallas_call(functools.partial(kernel, Z, T), out_shape=(pltpu.VMEM((4,...]
    unnamed x31 -> x0, local copies, waits for them, and re-layouts: 9.64 us -> none
    another operation x4 -> x0, other arithmetic: 2.54 us -> none  [the longest x2 1.71 us: on_device(): downs = jnp.stack([wd1.astype(bf), wd2.astype(bf)])]
where the time goes in v3:
time: 209 us; the launch traced here: 208 us
  Pallas kernels  207 us (99%)
    pallas_call x1, Pallas kernels, on_device(): pl.pallas_call(functools.partial(kernel, Z, T), out_shape=(pltpu.VMEM((4,...  205 us

profile of v3, /device:TPU:40, one launch (start us, length us, event | category | flops | bytes accessed | tf_op | source)
XLA Modules:
  0.0 208.0 jit_solution(10860295578066230508)
XLA Ops:
  0.6 205.3 %handoff.1 = (bf16[4,32,4,16,128]{4,3,2,1,0:T(8,128)(2,1)S(1)}, bf16[2,128,2048]{2,1,0:T(8,128)(2,1)S(1)}, bf16[256,2048]{1,0:T(8,128)(2,1)S(1)}) custom-call(bf16[256,2048]{1,0:T(8,128)(2,1)} %prompt_in.1, f32[1,64]{1,0:T(1,128)} %bitcast.6, f32[64,512]{1,0:T(8,128)} %wg1.1, f32[64,512]{1,0:T(8,128)} %wu1.1, f32[128,256]{1,0:T(8,128)} %wd1.1, ...), custom_call_target="tpu_custom_call" | custom-call | tf_op jit(solution)/shard_map/handoff/pallas_call | solution.py:337
  205.9 2.1 put_out.1

commit v4 on v3

--- a/solution.py
+++ b/solution.py
@@ -9,14 +9,15 @@
 
 EPS = 1e-06
 VMEM = 67_043_328
+NEAR = 4
 CORES = 2
 MESH = pl.DeviceIdType.MESH
-TREE = (0, 1, 0, 3, 4, 0)
-
-
-def tree(span):
-    K = len(TREE)
-    parent = {m: (m - 1) // K * K + TREE[(m - 1) % K] for m in range(1, span + 1)}
+TREES = ((0, 0, 0, 0), (0, 1, 0))
+
+
+def tree(span, shape):
+    K = len(shape)
+    parent = {m: (m - 1) // K * K + shape[(m - 1) % K] for m in range(1, span + 1)}
     feeds = {a: [m for m in range(span, 0, -1) if parent[m] == a] for a in range(span + 1)}
     starts = [a for a in range(0, span + 1, K) if feeds[a]]
     order = []
@@ -47,10 +48,10 @@
     prompt_in, g1, wg1, wu1, wd1, g2, wg2, wu2, wd2,
     C, DN, NX,
     prompt, gains, wide, tall, folded, downs,
-    A, B, part, R, S, N,
+    A, B, part, total, R, S, N,
     a_send, a_recv, b_send, b_recv, c_send, c_recv, p_recv, d_send, d_recv,
     r_send, r_recv, g_send, g_recv,
-    loc, load_sem,
+    loc, load_sem, word,
 ):
     z = lax.axis_index("fs")
     t = lax.axis_index("tp")
@@ -76,13 +77,13 @@
 
     barrier = pltpu.get_barrier_semaphore()
 
-    @pl.loop(1, Z)
-    def _(k):
-        pl.semaphore_signal(barrier, inc=1, device_id={"fs": lax.rem(z + k, Z)}, device_id_type=MESH)
-
-    @pl.loop(1, T)
-    def _(k):
-        pl.semaphore_signal(barrier, inc=1, device_id={"tp": lax.rem(t + k, T)}, device_id_type=MESH)
+    def near(r):
+        return [{"fs": lax.rem(z + k, Z)} for k in (r, Z - r)]
+
+    first = sorted({k for r in range(1, NEAR + 1) for k in (r, Z - r)})
+
+    for where in [{"fs": lax.rem(z + k, Z)} for k in first] + [{"tp": lax.rem(t + k, T)} for k in range(1, T)]:
+        pl.semaphore_signal(barrier, inc=1, device_id=where, device_id_type=MESH)
 
     for layer in range(2):
         for k in range(1, 4):
@@ -94,6 +95,54 @@
     for layer in range(2):
         loads[4 * layer + 4].wait()
         downs[layer] = tall[layer].astype(jnp.bfloat16)
+    pl.semaphore_wait(barrier, len(first) + T - 1)
+
+    radii = [NEAR << k for k in range(H.bit_length()) if NEAR << k < H]
+
+    def tell(k):
+        for where in near(radii[k]):
+            pl.semaphore_signal(word.at[k], inc=1, device_id=where, device_id_type=MESH)
+
+    if radii:
+        tell(0)
+
+    pend = {}
+
+    def due(name, ref, sem):
+        pend[name] = lambda: wait_bytes(ref, sem)
+
+    def settle(name):
+        pend.pop(name)()
+
+    def finish():
+        for name in list(pend):
+            settle(name)
+
+    def slice_of(layer, tt):
+        return folded.at[2 * layer + tt // X, pl.ds(pl.multiple_of(lax.rem(tt, X) * rq, rq), rq), :]
+
+    for layer in range(2):
+        @pl.loop(1, T)
+        def _(k):
+            tt = lax.rem(t + k, T)
+            rcopy(slice_of(layer, tt), A.at[layer, t], a_send.at[layer], a_recv.at[layer], tp=tt).start()
+
+        pltpu.make_async_copy(slice_of(layer, t), A.at[layer, t], a_recv.at[layer]).start()
+        due(f"A{layer}", A.at[layer], a_recv.at[layer])
+        due(f"As{layer}", A.at[layer, pl.ds(0, T - 1)], a_send.at[layer])
+
+    for layer in range(2):
+        mine = DN.at[layer, :, pl.ds(pl.multiple_of(t * dcol, dcol), dcol)]
+
+        @pl.loop(1, T)
+        def _(k):
+            tt = lax.rem(t + k, T)
+            rcopy(downs.at[layer], mine, d_send.at[layer], d_recv.at[layer], tp=tt).start()
+
+        pltpu.make_async_copy(downs.at[layer], mine, d_recv.at[layer]).start()
+        due(f"D{layer}", DN.at[layer], d_recv.at[layer])
+        due(f"Ds{layer}", DN.at[layer, :, pl.ds(0, (T - 1) * dcol)], d_send.at[layer])
+
     loads[0].wait()
 
     @pl.loop(0, tok // 16)
@@ -106,44 +155,10 @@
     stream = jnp.where(lax.rem(z, 2) == 0, pair[:own], pair[own:])
     stream = jnp.concatenate([stream[:, :half], stream[:, half:]], axis=0)
 
-    pl.semaphore_wait(barrier, Z + T - 2)
-
-    pend = {}
-
-    def due(name, ref, sem):
-        pend[name] = lambda: wait_bytes(ref, sem)
-
-    def settle(name):
-        pend.pop(name)()
-
-    def finish():
-        for name in list(pend):
-            settle(name)
-
-    def slice_of(layer, tt):
-        return folded.at[2 * layer + tt // X, pl.ds(pl.multiple_of(lax.rem(tt, X) * rq, rq), rq), :]
-
-    for layer in range(2):
-        @pl.loop(1, T)
-        def _(k):
-            tt = lax.rem(t + k, T)
-            rcopy(slice_of(layer, tt), A.at[layer, t], a_send.at[layer], a_recv.at[layer], tp=tt).start()
-
-        pltpu.make_async_copy(slice_of(layer, t), A.at[layer, t], a_recv.at[layer]).start()
-        due(f"A{layer}", A.at[layer], a_recv.at[layer])
-        due(f"As{layer}", A.at[layer, pl.ds(0, T - 1)], a_send.at[layer])
-
-    for layer in range(2):
-        mine = DN.at[layer, :, pl.ds(pl.multiple_of(t * dcol, dcol), dcol)]
-
-        @pl.loop(1, T)
-        def _(k):
-            tt = lax.rem(t + k, T)
-            rcopy(downs.at[layer], mine, d_send.at[layer], d_recv.at[layer], tp=tt).start()
-
-        pltpu.make_async_copy(downs.at[layer], mine, d_recv.at[layer]).start()
-        due(f"D{layer}", DN.at[layer], d_recv.at[layer])
-        due(f"Ds{layer}", DN.at[layer, :, pl.ds(0, (T - 1) * dcol)], d_send.at[layer])
+    for k in range(len(radii)):
+        pl.semaphore_wait(word.at[k], 2)
+        if k + 1 < len(radii):
+            tell(k + 1)
 
     def block_for(layer, zz):
         return A.at[layer, zz // zper, :, pl.ds(pl.multiple_of(lax.rem(zz, zper) * hid, hid), hid)]
@@ -165,11 +180,16 @@
     def rows_of(layer, tt):
         return C.at[2 * layer + tt // X, :, lax.rem(tt, X)]
 
+    around = X == 4
+
+    def half_of(layer, tt, h):
+        return C.at[2 * layer + tt // X, pl.ds(h * H, H), lax.rem(tt, X)]
+
     def gather_start(layer):
         settle(f"B{layer}")
-        for k in range(1, X):
+        for k in (1, X - 1) if around else range(1, X):
             tt = lax.rem(t + CORES * k, T)
-            rcopy(B.at[layer], rows_of(layer, t), c_send.at[layer], c_recv.at[layer, k - 1], tp=tt).start()
+            rcopy(B.at[layer], rows_of(layer, t), c_send.at[layer], c_recv.at[layer, k], tp=tt).start()
         rcopy(B.at[layer], rows_of(layer, t), c_send.at[layer], p_recv.at[layer], tp=partner).start()
         pltpu.make_async_copy(B.at[layer], rows_of(layer, t), loc.at[layer]).start()
         due(f"Cp{layer}", C.at[2 * layer], p_recv.at[layer])
@@ -178,10 +198,21 @@
         due(f"Ct{layer}", C.at[2 * layer, :, pl.ds(0, X - 1)], c_send.at[layer])
 
     def gather_pass(layer):
-        for k in (1, 3, 2) if X == 4 else range(1, X):
+        for k in (1, X - 1, 2) if around else range(1, X):
             tt = lax.rem(t + T - CORES * k, T)
-            pltpu.make_async_copy(rows_of(layer, tt), rows_of(layer, tt), c_recv.at[layer, k - 1]).wait()
-            rcopy(rows_of(layer, tt), rows_of(layer, tt), c_send.at[layer], p_recv.at[layer], tp=partner).start()
+            rows_tt = rows_of(layer, tt)
+            if around and k == 2:
+                for h in (0, 2):
+                    piece = half_of(layer, tt, h // 2)
+                    pltpu.make_async_copy(piece, piece, c_recv.at[layer, h]).wait()
+            else:
+                pltpu.make_async_copy(rows_tt, rows_tt, c_recv.at[layer, k]).wait()
+                if around:
+                    h = 0 if k == 1 else 1
+                    piece = half_of(layer, tt, h)
+                    on = lax.rem(t + (CORES if k == 1 else T - CORES), T)
+                    rcopy(piece, piece, c_send.at[layer], c_recv.at[layer, 2 * h], tp=on).start()
+            rcopy(rows_tt, rows_tt, c_send.at[layer], p_recv.at[layer], tp=partner).start()
 
     def gather_end(layer):
         settle(f"Cp{layer}")
@@ -202,8 +233,8 @@
     def at(side, m):
         return lax.rem(z + (Z - m if side == 0 else m), Z)
 
-    def reduce_scatter(layer):
-        trees = [tree(M) for M in reach]
+    def reduce_along(layer, shape):
+        trees = [tree(M, shape) for M in reach]
 
         def send(side, m, value):
             S[layer, side, m - 1] = value.astype(jnp.bfloat16)
@@ -236,14 +267,19 @@
             if a:
                 send(side, a, gathered(side, a))
                 own_sums(side, k + lead)
+        total[...] = gathered(0, 0) + gathered(1, 0) - part[z]
+
+    def reduce_scatter(layer):
+        for core, shape in enumerate(TREES):
+            pl.when(c == core)(functools.partial(reduce_along, layer, shape))
         for side in range(2):
             due(f"Rs{layer}{side}", S.at[layer, side, pl.ds(0, reach[side])], r_send.at[layer, side])
-        return gathered(0, 0) + gathered(1, 0) - part[z]
+        return total[...]
 
     span = (H - 1, H)
 
-    def all_gather(layer, beside):
-        trees = [tree(M) for M in span]
+    def gather_along(layer, shape):
+        trees = [tree(M, shape) for M in span]
 
         def arrived(side, m):
             slot = N.at[layer, at(side, m)]
@@ -257,12 +293,16 @@
                 rcopy(
                     slot, slot, g_send.at[layer, side], g_recv.at[layer, side, m - 1], fs=at(1 - side, m - a),
                 ).start()
-        beside()
         for side in range(2):
-            due(f"Gs{layer}{side}", N.at[layer, pl.ds(0, span[side])], g_send.at[layer, side])
             for m in range(1, span[side] + 1):
                 if not trees[side][1][m]:
                     arrived(side, m)
+
+    def all_gather(layer):
+        for core, shape in enumerate(TREES):
+            pl.when(c == core)(functools.partial(gather_along, layer, shape))
+        for side in range(2):
+            due(f"Gs{layer}{side}", N.at[layer, pl.ds(0, span[side])], g_send.at[layer, side])
 
     def in_rows(layer, out):
         @pl.loop(0, Z // 2)
@@ -291,21 +331,20 @@
     gather_pass(0)
     gather_end(0)
     partial_sums(0)
-    total = reduce_scatter(0)
-    stream = stream + 0.5 * total
+    gather_start(1)
+    stream = stream + 0.5 * reduce_scatter(0)
     mean = jnp.sum(stream * stream, axis=-1, keepdims=True)
     mean = (mean[:own] + mean[own:]) / D
     mean = jnp.concatenate([mean, mean], axis=0)
     N[0, z] = (stream * lax.rsqrt(mean + EPS)).astype(jnp.bfloat16)
-    gather_start(1)
-    all_gather(0, lambda: gather_pass(1))
+    gather_pass(1)
+    all_gather(0)
     in_rows(0, NX)
     gather_end(1)
     partial_sums(1)
-    total = reduce_scatter(1)
-    stream = stream + 0.5 * total
+    stream = stream + 0.5 * reduce_scatter(1)
     N[1, z] = stream.astype(jnp.bfloat16)
-    all_gather(1, lambda: None)
+    all_gather(1)
     in_rows(1, NX)
     finish()
 
@@ -349,11 +388,12 @@
             pltpu.VMEM((2, T, rq, width), bf),
             pltpu.VMEM((2, Z, rq, hid), bf),
             pltpu.VMEM((Z, 2 * own, D // 2), f32),
+            pltpu.VMEM(ring[3:], f32),
             pltpu.VMEM(ring, bf), pltpu.VMEM(ring, bf),
             pltpu.VMEM((2, Z, 2 * own, D // 2), bf),
-            dma((2,)), dma((2,)), dma((2,)), dma((2,)), dma((2,)), dma((2, X - 1)), dma((2,)), dma((2,)), dma((2,)),
+            dma((2,)), dma((2,)), dma((2,)), dma((2,)), dma((2,)), dma((2, X)), dma((2,)), dma((2,)), dma((2,)),
             dma((2, 2)), dma((2, 2, H)), dma((2, 2)), dma((2, 2, H)),
-            dma((2,)), dma((9,)),
+            dma((2,)), dma((9,)), pltpu.SemaphoreType.REGULAR((H.bit_length(),)),
         ],
         compiler_params=pltpu.CompilerParams(collective_id=0, has_side_effects=True, vmem_limit_bytes=VMEM - 2 * (4 * Z * X * rq * hid + 2 * hid * D + tok * D)),
         name="handoff",

time: 209 us -> 204 us (0.976)
  Pallas kernels: 207 us -> 200 us
    pallas_call x1, Pallas kernels: 205 us -> 198 us  [on_device(): pl.pallas_call(functools.partial(kernel, Z, T), out_shape=(pltpu.VMEM((4,...]
where the time goes in v4:
time: 204 us; the launch traced here: 201 us
  Pallas kernels  200 us (98%)
    pallas_call x1, Pallas kernels, on_device(): pl.pallas_call(functools.partial(kernel, Z, T), out_shape=(pltpu.VMEM((4,...  198 us

profile of v4, /device:TPU:40, one launch (start us, length us, event | category | flops | bytes accessed | tf_op | source)
XLA Modules:
  0.0 200.9 jit_solution(6399075099334701890)
XLA Ops:
  0.6 198.2 %handoff.1 = (bf16[4,32,4,16,128]{4,3,2,1,0:T(8,128)(2,1)S(1)}, bf16[2,128,2048]{2,1,0:T(8,128)(2,1)S(1)}, bf16[256,2048]{1,0:T(8,128)(2,1)S(1)}) custom-call(bf16[256,2048]{1,0:T(8,128)(2,1)} %prompt_in.1, f32[1,64]{1,0:T(1,128)} %bitcast.6, f32[64,512]{1,0:T(8,128)} %wg1.1, f32[64,512]{1,0:T(8,128)} %wu1.1, f32[128,256]{1,0:T(8,128)} %wd1.1, ...), custom_call_target="tpu_custom_call" | custom-call | tf_op jit(solution)/shard_map/handoff/pallas_call | solution.py:376
  198.9 2.1 %put_out.1 = (bf16[256,2048]{1,0:T(8,128)(2,1)}, bf16[32,4,16,128]{3,2,1,0:T(8,128)(2,1)}, bf16[32,4,16,128]{3,2,1,0:T(8,128)(2,1)}, bf16[128,2048]{1,0:T(8,128)...) custom-call(bf16[4,32,4,16,128]{4,3,2,1,0:T(8,128)(2,1)S(1)} %get-tuple-element, ...), custom_call_target="tpu_custom_call" | custom-call | tf_op jit(solution)/shard_map/put_out/pallas_call | solution.py:401
